TPU v7x, 32 devices: a whole 2x2x4 slice. The times are simulated.
32 devices in a mesh: ep: 8 (over z, x), tp: 4 (over y, core).
Axes of the slice: x: 2, y: 2, z: 4, core: 2. Of those that a mesh axis runs over, the one named last changes fastest.
Arguments:
- tokens: bfloat16 [1024, 2048], P('ep'), may hold values from -16 to 16
- routes: int32 [1024, 2], P('ep'), may hold values from 0 to 7, all different within a row; in each aligned block of 128 rows (0 to 127, 128 to 255, ...) at most 48 rows name the same one
- router: bfloat16 [2048, 8], replicated, may hold values from -0.125 to 0.125
- w_gate: bfloat16 [8, 2048, 2048], P('ep', None, 'tp'), may hold values from -0.125 to 0.125
- w_up: bfloat16 [8, 2048, 2048], P('ep', None, 'tp'), may hold values from -0.125 to 0.125
- w_down: bfloat16 [8, 2048, 2048], P('ep', 'tp'), may hold values from -0.125 to 0.125
- cotangent: bfloat16 [1024, 2048], P('ep'), may hold values from -6 to 6
Outputs:
- grad_tokens: bfloat16 [1024, 2048], P('ep', 'tp')
- grad_router: float32 [2048, 8], P('tp')
- grad_gate: float32 [8, 2048, 2048], P('ep', None, 'tp')
- grad_up: float32 [8, 2048, 2048], P('ep', None, 'tp')
- grad_down: float32 [8, 2048, 2048], P('ep', 'tp')
Inputs may be any that keep to these rules, and one draw needn't show every extreme that they name: In each aligned block of 128 rows, no expert is named by more than 48 of the block's routes, a bound that some block reaches; a row names 2 different experts.
All inputs are finite; a program needn't handle non-finite values.
Results may differ from a plain program's by a relative error of at most 0.017.
Values may be sent and summed in bfloat16 or wider, within the bound.
A program may use at most 128 MiB of HBM per device.

v0:
```python
import jax
import jax.numpy as jnp
from jax import lax
from jax.sharding import PartitionSpec as P

clamp_limit = 7.0
sig_slope = 1.702


def on_device(tokens, routes, router, w_gate, w_up, w_down, cotangent):
    highest = lax.Precision.HIGHEST
    ep_count = lax.axis_size("ep")
    tp_count = lax.axis_size("tp")
    tp_index = lax.axis_index("tp")
    tok_rows = tokens.shape[0]
    model_width = tokens.shape[1]
    top_count = routes.shape[1]
    local_experts = w_gate.shape[0]
    all_experts = ep_count * local_experts
    capacity = 3 * tok_rows * top_count // (2 * all_experts)
    slot_count = all_experts * capacity
    feature_part = model_width // tp_count
    feature_start = tp_index * feature_part
    buffer_shape = (ep_count, local_experts, capacity)
    logits = jnp.dot(tokens, router, preferred_element_type=jnp.float32)
    expert_hot = routes[:, :, None] == jnp.arange(all_experts, dtype=jnp.int32)[None, None, :]
    chosen = jnp.sum(jnp.where(expert_hot, logits[:, None, :], 0.0), axis=2)
    weights = 1.0 / jnp.sum(jnp.exp(chosen[:, None, :] - chosen[:, :, None]), axis=2)
    flat_hot = expert_hot.reshape(tok_rows * top_count, all_experts).astype(jnp.int32)
    earlier = jnp.cumsum(flat_hot, axis=0) - flat_hot
    position = jnp.sum(earlier * flat_hot, axis=1).reshape(tok_rows, top_count)
    slot_of = routes * capacity + position
    select = slot_of[None, :, :] == jnp.arange(slot_count, dtype=jnp.int32)[:, None, None]
    dispatch = jnp.any(select, axis=2)
    dispatch_half = dispatch.astype(jnp.bfloat16)
    slot_weight = jnp.sum(jnp.where(select, weights[None, :, :], 0.0), axis=(1, 2))
    token_cols = lax.dynamic_slice_in_dim(tokens, feature_start, feature_part, 1)
    cot_cols = lax.dynamic_slice_in_dim(cotangent, feature_start, feature_part, 1)
    token_slots = jnp.dot(dispatch_half, token_cols, preferred_element_type=jnp.float32).astype(
        jnp.bfloat16
    )
    cot_slots = jnp.dot(dispatch_half, cot_cols, preferred_element_type=jnp.float32).astype(
        jnp.bfloat16
    )
    scaled = (slot_weight[:, None] * cot_slots).astype(jnp.bfloat16)
    sent_tok, sent_cot = (
        lax.all_to_all(
            token_slots.reshape(buffer_shape + (feature_part,)),
            "ep",
            split_axis=0,
            concat_axis=0,
            tiled=True,
        ),
        lax.all_to_all(
            scaled.reshape(buffer_shape + (feature_part,)),
            "ep",
            split_axis=0,
            concat_axis=0,
            tiled=True,
        ),
    )
    arrived, arrived_cot = (
        lax.all_gather(sent_tok, "tp", axis=3, tiled=True),
        lax.all_gather(sent_cot, "tp", axis=3, tiled=True),
    )
    pre_gate = jnp.einsum("slcd,ldf->slcf", arrived, w_gate, preferred_element_type=jnp.float32)
    pre_up = jnp.einsum("slcd,ldf->slcf", arrived, w_up, preferred_element_type=jnp.float32)
    gate_clamped = jnp.minimum(pre_gate, clamp_limit)
    up_clamped = jnp.clip(pre_up, -clamp_limit, clamp_limit)
    sigmoid_gate = jax.nn.sigmoid(sig_slope * gate_clamped)
    gated_act = gate_clamped * sigmoid_gate
    activation = ((up_clamped + 1.0) * gated_act).astype(jnp.bfloat16)
    back_act = jnp.einsum("slcd,lfd->slcf", arrived_cot, w_down, preferred_element_type=jnp.float32)
    share_part = jnp.sum(activation.astype(jnp.float32) * back_act, axis=3)
    slope_term = sigmoid_gate + sig_slope * gated_act * (1.0 - sigmoid_gate)
    d_gate = jnp.where(
        pre_gate < clamp_limit, back_act * (up_clamped + 1.0) * slope_term, 0.0
    ).astype(jnp.bfloat16)
    d_up = jnp.where(jnp.abs(pre_up) < clamp_limit, back_act * gated_act, 0.0).astype(jnp.bfloat16)
    grad_gate = jnp.einsum("slcd,slcf->ldf", arrived, d_gate, preferred_element_type=jnp.float32)
    grad_up = jnp.einsum("slcd,slcf->ldf", arrived, d_up, preferred_element_type=jnp.float32)
    grad_down = jnp.einsum(
        "slcf,slcd->lfd", activation, arrived_cot, preferred_element_type=jnp.float32
    )
    row_term = jnp.einsum("ldf,slcf->dslc", w_gate, d_gate, preferred_element_type=jnp.float32)
    input_part = lax.psum_scatter(
        (
            row_term + jnp.einsum("ldf,slcf->dslc", w_up, d_up, preferred_element_type=jnp.float32)
        ).astype(jnp.bfloat16),
        "tp",
        scatter_dimension=0,
        tiled=True,
    ).astype(jnp.float32)
    share_sum = lax.psum(share_part, "tp")
    back_input, back_share = (
        lax.all_to_all(
            input_part.astype(jnp.bfloat16), "ep", split_axis=1, concat_axis=1, tiled=True
        ).astype(input_part.dtype),
        lax.all_to_all(
            share_sum[None].astype(jnp.bfloat16), "ep", split_axis=1, concat_axis=1, tiled=True
        ).astype(jnp.float32),
    )
    back_input = back_input.reshape(feature_part, slot_count)
    back_share = back_share.reshape(slot_count)
    dispatch_full = dispatch.astype(jnp.float32)
    from_experts = lax.dot_general(
        dispatch_full, back_input, (((0,), (1,)), ((), ())), precision=highest
    )
    shares = jnp.sum(jnp.where(select, back_share[:, None, None], 0.0), axis=0)
    mixed_grad = shares - weights * jnp.sum(shares, axis=1, keepdims=True)
    d_logits = jnp.sum(jnp.where(expert_hot, mixed_grad[:, :, None], 0.0), axis=1)
    router_rows = lax.dynamic_slice_in_dim(router, feature_start, feature_part, 0).astype(
        jnp.float32
    )
    from_router = lax.dot_general(
        d_logits, router_rows, (((1,), (1,)), ((), ())), precision=highest
    )
    grad_tokens = (from_experts + from_router).astype(jnp.bfloat16)
    router_part = lax.dot_general(
        token_cols.astype(jnp.float32), d_logits, (((0,), (0,)), ((), ())), precision=highest
    )
    grad_router = lax.psum(router_part, "ep")
    return (grad_tokens, grad_router, grad_gate, grad_up, grad_down)


def solution(mesh):
    return jax.shard_map(
        on_device,
        mesh=mesh,
        in_specs=(
            P("ep", None),
            P("ep", None),
            P(),
            P("ep", None, "tp"),
            P("ep", None, "tp"),
            P("ep", "tp", None),
            P("ep", None),
        ),
        out_specs=(
            P("ep", "tp"),
            P("tp", None),
            P("ep", None, "tp"),
            P("ep", None, "tp"),
            P("ep", "tp", None),
        ),
        check_vma=False,
    )
```

profile of v0, /device:TPU:0, one launch (start us, length us, event | category | flops | bytes accessed | tf_op | source)
XLA Modules:
  0.0 159.0 jit_solution(8178199809806928618)
XLA Ops:
  7.2 0.0 copy-start
  7.2 0.0 copy-start.4
  7.2 0.0 copy-start.2
  7.2 0.0 copy-start.3
  7.2 0.0 all-gather.3.cloned.1.call-start
  7.3 0.9 copy.55
  8.2 0.1 eq.49
  8.3 0.1 eq.45
  8.5 0.6 reduce-window.6
  9.1 0.2 slice_reduce_fusion
  9.3 0.1 fusion.44
  9.4 0.1 reshape.140
  9.6 0.1 copy.57
  9.6 0.7 multiply_add_fusion
  10.4 1.2 convolution_convert_fusion.1
  11.6 19.2 %all_to_all.20 = bf16[8,1,48,512]{3,2,1,0:T(8,128)(2,1)} all-to-all(bf16[8,1,48,512]{3,2,1,0:T(8,128)(2,1)S(1)} %bitcast.163), channel_id=1, replica_groups=mesh['ep'=8,'tp'=4] {'ep'}, dimensions={0} | all-to-all | bytes 786432 | tf_op jit(solution)/shard_map/all_to_all | solution.py:47
  30.8 0.0 all-gather.3.cloned.1.call-update
  30.8 0.0 all-gather.5.cloned.1.call-start
  30.9 0.0 copy-done.2
  30.9 0.0 copy-done.3
  30.9 0.2 fusion.57
  31.1 0.0 copy-done.4
  31.2 0.2 select_reduce_fusion.2
  31.4 1.2 fusion.23
  32.5 15.1 %all_to_all.21 = bf16[8,1,48,512]{3,2,1,0:T(8,128)(2,1)} all-to-all(bf16[8,1,48,512]{3,2,1,0:T(8,128)(2,1)S(1)} %bitcast.162), channel_id=1, replica_groups=mesh['ep'=8,'tp'=4] {'ep'}, dimensions={0} | all-to-all | bytes 786432 | tf_op jit(solution)/shard_map/all_to_all | solution.py:54
  47.6 0.0 all-gather.5.cloned.1.call-update
  47.6 0.0 reduce-scatter.2.cloned.1.call-start
  47.7 1.6 %all-gather.3.cloned.1.call-done = bf16[8,1,48,2048]{3,2,0,1:T(8,128)(2,1)} async-done(((bf16[8,1,48,512]{3,2,0,1:T(8,128)(2,1)}), bf16[8,1,48,2048]{3,2,0,1:T(8,128)(2,1)}) %all-gather.3.cloned.1.call-update) | async-done | bytes 1572880 | tf_op jit(solution)/shard_map/all_gather | solution.py:63
  49.3 0.0 copy-start.5
  49.3 4.0 %fusion.2 = f32[8,48,512]{2,1,0:T(8,128)} fusion(bf16[1,2048,512]{2,1,0:T(8,128)(2,1)} %param.11, bf16[8,1,48,2048]{3,2,0,1:T(8,128)(2,1)} %all-gather.3.cloned.1.call-done), kind=kOutput, calls=%fused_computation.6 | convolution fusion | flops 805306368 | bytes 4456448 | tf_op jit(solution)/shard_map/slcd,ldf->slcf/dot_general | solution.py:67
  53.4 0.0 copy-done
  53.4 0.0 copy-done.5
  53.4 1.9 %fusion.8 = f32[8,48,512]{2,1,0:T(8,128)} fusion(bf16[1,2048,512]{2,1,0:T(8,128)(2,1)S(1)} %copy-done, bf16[8,1,48,2048]{3,2,0,1:T(8,128)(2,1)S(1)} %copy-done.5), kind=kOutput, calls=%fused_computation.12 | convolution fusion | flops 805306368 | bytes 4456448 | tf_op jit(solution)/shard_map/slcd,ldf->slcf/dot_general | solution.py:66
  55.2 15.3 %all-gather.5.cloned.1.call-done = bf16[8,1,48,2048]{3,2,0,1:T(8,128)(2,1)} async-done(((bf16[8,1,48,512]{3,2,0,1:T(8,128)(2,1)}), bf16[8,1,48,2048]{3,2,0,1:T(8,128)(2,1)}) %all-gather.5.cloned.1.call-update) | async-done | bytes 1572880 | tf_op jit(solution)/shard_map/all_gather | solution.py:64
  70.5 4.7 %multiply_reduce_fusion = (f32[8,48]{1,0:T(8,128)S(1)}, bf16[8,1,48,512]{3,2,0,1:T(8,128)(2,1)}, bf16[8,48,512]{2,1,0:T(8,128)(2,1)S(1)}, bf16[8,1,48,512]{3,2,0,1:T(8,128)(2,1)S(1)}) fusion(f32[8,48,512]{2,1,0:T(8,128)} %fusion.8, f32[8,48,512]{2,1,0:T(8,128)} %fusion.2, bf16[1,512,2048]{2,1,0:T(8,128)(2,1)} %param.12, ...), kind=kOutput, calls=%fused_computation.40 | convolution fusion | flops 810614400 | bytes 6424064 | tf_op jit(solution)/shard_map/slcd,lfd->slcf/dot_general | solution.py:73
  75.3 0.0 copy-start.1
  75.3 1.0 fusion.6
  76.3 0.5 copy-done.1
  76.9 2.2 %fusion = bf16[2048,8,1,48]{0,3,1,2:T(8,128)(2,1)} fusion(f32[8,48,2048]{2,1,0:T(8,128)S(1)} %fusion.6, bf16[8,48,512]{2,1,0:T(8,128)(2,1)S(1)} %get-tuple-element.9, bf16[1,2048,512]{2,1,0:T(8,128)(2,1)S(1)} %copy-done.1), kind=kOutput, calls=%fused_computation.4 | convolution fusion | flops 806879232 | bytes 7208960 | tf_op jit(solution)/shard_map/ldf,slcf->dslc/dot_general | solution.py:88
  79.1 0.0 reduce-scatter.2.cloned.1.call-update
  79.1 5.9 %psum.14 = bf16[8,1,48]{2,0,1:T(8,128)(2,1)S(1)} all-reduce(f32[8,1,48]{2,0,1:T(8,128)S(1)} %bitcast.166), channel_id=1, replica_groups=mesh['ep'=8,'tp'=4] {'tp'}, use_global_device_ids=true, to_apply=%region_9.10 | all-reduce | flops 384 | bytes 2304 | tf_op jit(solution)/shard_map/psum | solution.py:94
  85.0 0.6 copy.63
  85.6 5.7 %all-to-all-start.3 = ((bf16[1,8,1,48]{3,2,0,1:T(2,128)(2,1)}), bf16[1,8,1,48]{3,2,0,1:T(2,128)(2,1)S(1)}, u32[]{:S(2)}, u32[]{:S(2)}) async-start(bf16[1,8,1,48]{3,2,0,1:T(2,128)(2,1)} %copy.63), calls=%async_computation.4 | async-start | bytes 8192 | tf_op jit(solution)/shard_map/all_to_all | solution.py:99
  91.3 0.0 copy-start.6
  91.3 4.8 %convolution_bitcast_fusion.1 = f32[1,2048,512]{2,1,0:T(8,128)} fusion(bf16[8,48,512]{2,1,0:T(8,128)(2,1)S(1)} %get-tuple-element.9, bf16[8,1,48,2048]{3,2,0,1:T(8,128)(2,1)} %all-gather.3.cloned.1.call-done), kind=kOutput, calls=%fused_computation.1 | convolution fusion | flops 805306368 | bytes 6160384 | tf_op jit(solution)/shard_map/slcd,slcf->ldf/dot_general | solution.py:81
  96.1 0.0 copy-done.6
  96.1 0.0 copy-start.7
  96.1 0.0 copy-start.8
  96.1 3.3 %convolution_bitcast_fusion.2 = f32[1,2048,512]{2,1,0:T(8,128)} fusion(bf16[8,1,48,2048]{3,2,0,1:T(8,128)(2,1)S(1)} %copy-done.6, bf16[8,1,48,512]{3,2,0,1:T(8,128)(2,1)S(1)} %get-tuple-element.10), kind=kOutput, calls=%fused_computation.2 | convolution fusion | flops 805306368 | bytes 6160384 | tf_op jit(solution)/shard_map/slcd,slcf->ldf/dot_general | solution.py:80
  99.5 0.0 copy-done.7
  99.5 0.0 copy-done.8
  99.5 3.3 %convolution_bitcast_fusion = f32[1,512,2048]{2,1,0:T(8,128)} fusion(bf16[8,1,48,2048]{3,2,0,1:T(8,128)(2,1)S(1)} %copy-done.7, bf16[8,1,48,512]{3,2,0,1:T(8,128)(2,1)S(1)} %copy-done.8), kind=kOutput, calls=%fused_computation | convolution fusion | flops 805306368 | bytes 6160384 | tf_op jit(solution)/shard_map/slcf,slcd->lfd/dot_general | solution.py:82
  102.8 0.0 all-to-all-done.3
  102.8 0.1 reshape.152
  102.9 0.2 select_reduce_fusion
  103.1 4.2 %reduce-scatter.2.cloned.1.call-done = bf16[512,8,1,48]{0,3,1,2:T(8,128)(2,1)} async-done(((bf16[2048,8,1,48]{0,3,1,2:T(8,128)(2,1)}), bf16[512,8,1,48]{0,3,1,2:T(8,128)(2,1)}) %reduce-scatter.2.cloned.1.call-update) | async-done | bytes 393232 | tf_op jit(solution)/shard_map/reduce_scatter | solution.py:86
  107.3 5.5 %all-to-all-start.2 = ((bf16[512,8,1,48]{0,3,2,1:T(8,128)(2,1)}), bf16[512,8,1,48]{0,3,2,1:T(8,128)(2,1)S(1)}, u32[]{:S(2)}, u32[]{:S(2)}) async-start(bf16[512,8,1,48]{0,3,2,1:T(8,128)(2,1)} %bitcast.164), calls=%async_computation.3 | async-start | bytes 786432 | tf_op jit(solution)/shard_map/all_to_all | solution.py:96
  112.8 0.2 fusion.40
  113.0 38.3 %psum.15 = f32[512,8]{0,1:T(8,128)} all-reduce(f32[512,8]{0,1:T(8,128)S(1)} %fusion.40), channel_id=1, replica_groups=mesh['ep'=8,'tp'=4] {'ep'}, use_global_device_ids=true, to_apply=%region_13.14 | all-reduce | flops 4096 | bytes 32768 | tf_op jit(solution)/shard_map/psum | solution.py:122
  151.2 0.3 fusion.45
  151.5 0.0 all-to-all-done.2
  151.6 0.9 fusion.24
  (10 shorter events, 0.2 us)
Async XLA Ops:
  7.2 46.2 %copy-start = (bf16[1,2048,512]{2,1,0:T(8,128)(2,1)S(1)}, bf16[1,2048,512]{2,1,0:T(8,128)(2,1)}, u32[]{:S(2)}) copy-start(bf16[1,2048,512]{2,1,0:T(8,128)(2,1)} %param.10) | copy-start | bytes 6291460
  7.2 24.0 %copy-start.4 = (s32[128,2]{0,1:T(2,128)S(1)}, s32[128,2]{0,1:T(2,128)}, u32[]{:S(2)}) copy-start(s32[128,2]{0,1:T(2,128)} %param.8) | copy-start | bytes 3076
  7.2 23.7 %copy-start.2 = (bf16[128,2048]{1,0:T(8,128)(2,1)S(1)}, bf16[128,2048]{1,0:T(8,128)(2,1)}, u32[]{:S(2)}) copy-start(bf16[128,2048]{1,0:T(8,128)(2,1)} %param.7) | copy-start | bytes 1572868
  7.2 23.7 %copy-start.3 = (bf16[2048,8]{0,1:T(8,128)(2,1)S(1)}, bf16[2048,8]{0,1:T(8,128)(2,1)}, u32[]{:S(2)}) copy-start(bf16[2048,8]{0,1:T(8,128)(2,1)} %param.9) | copy-start | bytes 98308
  7.2 42.1 %all-gather.3.cloned.1.call-start = ((), (), s32[]{:S(2)}) async-start(), calls=%async_computation.5 | async-start | bytes 1966080 | tf_op jit(solution)/shard_map/all_gather | solution.py:63
  30.8 39.7 %all-gather.5.cloned.1.call-start = ((), (), s32[]{:S(2)}) async-start(), calls=%async_computation.6 | async-start | bytes 1966080 | tf_op jit(solution)/shard_map/all_gather | solution.py:64
  47.6 59.6 %reduce-scatter.2.cloned.1.call-start = ((), (), s32[]{:S(2)}) async-start(), calls=%async_computation.7 | async-start | bytes 1966080 | tf_op jit(solution)/shard_map/reduce_scatter | solution.py:86
  49.3 4.0 %copy-start.5 = (bf16[8,1,48,2048]{3,2,0,1:T(8,128)(2,1)S(1)}, bf16[8,1,48,2048]{3,2,0,1:T(8,128)(2,1)}, u32[]{:S(2)}) copy-start(bf16[8,1,48,2048]{3,2,0,1:T(8,128)(2,1)} %all-gather.3.cloned.1.call-done) | copy-start | bytes 4718596
  75.3 1.6 %copy-start.1 = (bf16[1,2048,512]{2,1,0:T(8,128)(2,1)S(1)}, bf16[1,2048,512]{2,1,0:T(8,128)(2,1)}, u32[]{:S(2)}) copy-start(bf16[1,2048,512]{2,1,0:T(8,128)(2,1)} %param.11) | copy-start | bytes 6291460
  85.6 17.2 %all-to-all-start.3 = ((bf16[1,8,1,48]{3,2,0,1:T(2,128)(2,1)}), bf16[1,8,1,48]{3,2,0,1:T(2,128)(2,1)S(1)}, u32[]{:S(2)}, u32[]{:S(2)}) async-start(bf16[1,8,1,48]{3,2,0,1:T(2,128)(2,1)} %copy.63), calls=%async_computation.4 | async-start | bytes 8192 | tf_op jit(solution)/shard_map/all_to_all | solution.py:99
  91.3 4.9 %copy-start.6 = (bf16[8,1,48,2048]{3,2,0,1:T(8,128)(2,1)S(1)}, bf16[8,1,48,2048]{3,2,0,1:T(8,128)(2,1)}, u32[]{:S(2)}) copy-start(bf16[8,1,48,2048]{3,2,0,1:T(8,128)(2,1)} %all-gather.3.cloned.1.call-done) | copy-start | bytes 4718596
  96.1 3.3 %copy-start.7 = (bf16[8,1,48,2048]{3,2,0,1:T(8,128)(2,1)S(1)}, bf16[8,1,48,2048]{3,2,0,1:T(8,128)(2,1)}, u32[]{:S(2)}) copy-start(bf16[8,1,48,2048]{3,2,0,1:T(8,128)(2,1)} %all-gather.5.cloned.1.call-done) | copy-start | bytes 4718596
  96.1 3.3 %copy-start.8 = (bf16[8,1,48,512]{3,2,0,1:T(8,128)(2,1)S(1)}, bf16[8,1,48,512]{3,2,0,1:T(8,128)(2,1)}, u32[]{:S(2)}) copy-start(bf16[8,1,48,512]{3,2,0,1:T(8,128)(2,1)} %get-tuple-element.8) | copy-start | bytes 1179652
  107.3 44.3 %all-to-all-start.2 = ((bf16[512,8,1,48]{0,3,2,1:T(8,128)(2,1)}), bf16[512,8,1,48]{0,3,2,1:T(8,128)(2,1)S(1)}, u32[]{:S(2)}, u32[]{:S(2)}) async-start(bf16[512,8,1,48]{0,3,2,1:T(8,128)(2,1)} %bitcast.164), calls=%async_computation.3 | async-start | bytes 786432 | tf_op jit(solution)/shard_map/all_to_all | solution.py:96
Sparse Core Ops, SparseCore 0:
  30.9 18.3 all-gather.2
  50.9 19.6 all-gather.4
  79.2 27.9 reduce-scatter.1
where the time goes:
time: 159 us
  blocking collectives  78.5 us (49%)
  matrix products  29.4 us (18%)
  waiting for transfers between devices  21.2 us (13%)
  between operations  13.9 us (9%)
  starting transfers between devices  11.3 us (7%)
  local copies, waits for them, and re-layouts  2.9 us (2%)
  other arithmetic  1.9 us (1%)
    psum x1, blocking collectives, on_device(): grad_router = lax.psum(router_part, 'ep')  38.3 us
    all_to_all x1, blocking collectives, on_device(): lax.all_to_all(token_slots.reshape(buffer_shape + (feature_part,)), 'ep',...  19.2 us
    all_gather x1, waiting for transfers between devices, on_device(): lax.all_gather(sent_cot, 'tp', axis=3, tiled=True)  15.3 us
    all_to_all x1, blocking collectives, on_device(): lax.all_to_all(scaled.reshape(buffer_shape + (feature_part,)), 'ep', spli...  15.1 us
    psum x1, blocking collectives, on_device(): share_sum = lax.psum(share_part, 'tp')  5.89 us
    all_to_all x1, starting transfers between devices, on_device(): lax.all_to_all(share_sum[None].astype(jnp.bfloat16), 'ep', split_axis=1,...  5.67 us
    all_to_all x1, starting transfers between devices, on_device(): lax.all_to_all(input_part.astype(jnp.bfloat16), 'ep', split_axis=1, conca...  5.51 us
    dot_general x1, matrix products, on_device(): jnp.einsum('slcd,slcf->ldf', arrived, d_up, preferred_element_type=jnp.fl...  4.85 us
  transfers between devices with their start and end apart: 5, of which 3 were waited for; matrix products, arithmetic and copies ran while one was open for 13% of the time, Pallas kernels for 0%

commit v1 on v0

v1 whole, which is shorter than its diff:
```python
import functools

import jax
import jax.numpy as jnp
from jax import lax
from jax.experimental import pallas as pl
from jax.experimental.pallas import tpu as pltpu
from jax.sharding import PartitionSpec as P

clamp_limit = 7.0
sig_slope = 1.702
MESH = pl.DeviceIdType.MESH
HIGH = lax.Precision.HIGHEST
NT = (((1,), (1,)), ((), ()))


def kernel(
    sizes,
    tok, rt, rout, cot, wg_hbm, wu_hbm, wd_hbm,
    gtok_out, grt_out, rows_out, cots_out, act_out, dg_out, du_out,
    wg, wu, wd, dsp, tok_send, cot_send, rows, cots, act, dg, du,
    part, cxr, ysend, yxr, ret_send, ret_recv,
    sh_part, shx, sh_tot, shr, rp_part, rpr,
    w_sem, o_sem, ep_s, ep_r, y_s, y_r, c_s, c_r,
    ca_s, ca_r, yb_s, yb_r, rb_s, rb_r, sa_s, sa_r, sb_s, sb_r, rp_s, rp_r,
):
    E, NTP, NY, C, T, D, F, H, groups = sizes
    me, tp = lax.axis_index("ep"), lax.axis_index("tp")
    y, c = tp // 2, lax.rem(tp, 2)
    f32, bf16 = jnp.float32, jnp.bfloat16

    def remote(src, dst, s, r, ep, tpi):
        return pltpu.make_async_remote_copy(
            src_ref=src, dst_ref=dst, send_sem=s, recv_sem=r,
            device_id=(ep, tpi), device_id_type=MESH)

    def up_ep(k):
        return lax.rem(me + k, E)

    def down_ep(k):
        return lax.rem(me + (E - k), E)

    def y_at(j):
        return lax.rem(y + j, NY)

    def cols_of(t):
        return pl.ds(pl.multiple_of(t * F, F), F)

    weight_copies = [
        pltpu.make_async_copy(a, b, w_sem.at[i])
        for i, (a, b) in enumerate(((wg_hbm, wg), (wu_hbm, wu), (wd_hbm, wd)))]
    for cp in weight_copies:
        cp.start()
    barrier = pltpu.get_barrier_semaphore()
    for k in range(1, E):
        pl.semaphore_signal(barrier, inc=1, device_id=(up_ep(k), tp), device_id_type=MESH)
    for j in range(1, NTP):
        pl.semaphore_signal(barrier, inc=1, device_id=(me, lax.rem(tp + j, NTP)), device_id_type=MESH)

    eid = lax.rem(lax.broadcasted_iota(jnp.int32, (E, T), 0) + me, E)
    hot = eid == rt[0:1, :]
    for i in range(1, rt.shape[0]):
        hot = hot | (eid == rt[i:i + 1, :])
    upper = (lax.broadcasted_iota(jnp.int32, (T, T), 0)
             < lax.broadcasted_iota(jnp.int32, (T, T), 1))
    pos = jnp.dot(hot.astype(f32).astype(bf16), upper.astype(f32).astype(bf16),
                  preferred_element_type=f32)
    posm = jnp.where(hot, pos, -1.0)
    crow = lax.broadcasted_iota(jnp.int32, (C, T), 0).astype(f32)
    for k in range(E):
        dsp[k * C:(k + 1) * C, :] = jnp.where(posm[k:k + 1, :] == crow, 1.0, 0.0).astype(bf16)
    tok_cols = tok[:, cols_of(tp)]
    cot_cols = cot[:, cols_of(tp)]
    tok_send[...] = jnp.dot(dsp[...], tok_cols, preferred_element_type=f32).astype(bf16)

    pl.semaphore_wait(barrier, E - 1 + NTP - 1)
    sends = []

    def send(*args):
        cp = remote(*args)
        cp.start()
        sends.append(cp)

    def blk(k):
        return pl.ds(k * C, C)

    for k in range(1, E):
        send(tok_send.at[blk(k), :], rows.at[blk(k), cols_of(tp)],
             ep_s.at[0], ep_r.at[0, k], up_ep(k), tp)

    perm = (lax.broadcasted_iota(jnp.int32, (E, E), 1)
            == lax.rem(lax.broadcasted_iota(jnp.int32, (E, E), 0) + me, E)).astype(f32)
    rout_rel = jnp.dot(perm.astype(bf16), rout[...], preferred_element_type=f32).astype(bf16)
    logits = lax.dot_general(rout_rel, tok[...], NT, preferred_element_type=f32)
    top = jnp.max(jnp.where(hot, logits, -1e30), axis=0, keepdims=True)
    ex = jnp.where(hot, jnp.exp(jnp.minimum(logits - top, 0.0)), 0.0)
    weight = ex / jnp.sum(ex, axis=0, keepdims=True)
    wcols = []
    for k in range(E):
        wcols.append(jnp.sum(jnp.where(posm[k:k + 1, :] == crow, weight[k:k + 1, :], 0.0),
                             axis=1, keepdims=True))
    for k in list(range(1, E)):
        raw = jnp.dot(dsp[blk(k), :], cot_cols, preferred_element_type=f32)
        cot_send[blk(k), :] = (wcols[k] * raw).astype(bf16)
    for k in range(1, E):
        send(cot_send.at[blk(k), :], cots.at[blk(k), cols_of(tp)],
             ep_s.at[1], ep_r.at[1, k], up_ep(k), tp)
    rows[0:C, :] = jnp.dot(dsp[0:C, :], tok[...], preferred_element_type=f32).astype(bf16)
    cots[0:C, :] = (wcols[0] * jnp.dot(dsp[0:C, :], cot[...], preferred_element_type=f32)).astype(bf16)

    bufs = (rows, cots)
    srcs = (tok_send, cot_send)

    def arrive(k):
        for a in range(2):
            buf = bufs[a]
            here = buf.at[blk(k), cols_of(tp)]
            remote(srcs[a].at[blk(k), :], here, ep_s.at[a], ep_r.at[a, k], me, tp).wait_recv()
            for j in range(1, NY):
                send(here, here, y_s.at[0], y_r.at[a, k, j], me, y_at(j) * 2 + c)
            send(here, here, c_s.at[0], c_r.at[a, k, 0], me, y * 2 + (1 - c))

    def pass_on(k):
        for a in range(2):
            for j in range(1, NY):
                t = lax.rem(y + (NY - j), NY) * 2 + c
                here = bufs[a].at[blk(k), cols_of(t)]
                remote(here, here, y_s.at[0], y_r.at[a, k, j], me, tp).wait_recv()
                send(here, here, c_s.at[0], c_r.at[a, k, j], me, y * 2 + (1 - c))

    def complete(k):
        for a in range(2):
            for j in range(NY):
                t = lax.rem(y + (NY - j), NY) * 2 + (1 - c)
                here = bufs[a].at[blk(k), cols_of(t)]
                remote(here, here, c_s.at[0], c_r.at[a, k, j], me, tp).wait_recv()

    tile = min(H, 256)
    ones = jnp.ones((8, tile), f32)

    def experts(k0, k1):
        r = pl.ds(k0 * C, (k1 - k0) * C)
        sums = [jnp.zeros((8, C), f32) for _ in range(k0, k1)]
        for n in range(0, H, tile):
            cn = slice(n, n + tile)
            pre_gate = jnp.dot(rows[r, :], wg[:, cn], preferred_element_type=f32)
            pre_up = jnp.dot(rows[r, :], wu[:, cn], preferred_element_type=f32)
            back = lax.dot_general(cots[r, :], wd[cn, :], NT, preferred_element_type=f32)
            g = jnp.minimum(pre_gate, clamp_limit)
            u1 = jnp.clip(pre_up, -clamp_limit, clamp_limit) + 1.0
            sg = jax.nn.sigmoid(sig_slope * g)
            ga = g * sg
            a = (u1 * ga).astype(bf16)
            act[r, cn] = a
            prod = a.astype(f32) * back
            slope = sg + sig_slope * ga * (1.0 - sg)
            dg[r, cn] = jnp.where(pre_gate < clamp_limit, back * u1 * slope, 0.0).astype(bf16)
            du[r, cn] = jnp.where(jnp.abs(pre_up) < clamp_limit, back * ga, 0.0).astype(bf16)
            for i in range(k1 - k0):
                sums[i] = sums[i] + lax.dot_general(
                    ones, prod[i * C:(i + 1) * C, :], NT, precision=HIGH, preferred_element_type=f32)
        for i in range(k1 - k0):
            sh_part[k0 + i, :, 0:C] = sums[i]

    def row_term(g, k0, k1):
        r = pl.ds(k0 * C, (k1 - k0) * C)
        for n in range(0, D, 512):
            part[r, n:n + 512] = (
                lax.dot_general(dg[r, :], wg[n:n + 512, :], NT, preferred_element_type=f32)
                + lax.dot_general(du[r, :], wu[n:n + 512, :], NT, preferred_element_type=f32)
            ).astype(bf16)
        for j in range(NY):
            send(part.at[r, cols_of(y_at(j) * 2 + (1 - c))], cxr.at[r, j * F:(j + 1) * F],
                 ca_s.at[0], ca_r.at[g, j], me, y * 2 + (1 - c))

    def chip_sum(g, k0, k1):
        r = pl.ds(k0 * C, (k1 - k0) * C)
        for j in list(range(1, NY)) + [0]:
            remote(part.at[r, cols_of(y_at(j) * 2 + (1 - c))], cxr.at[r, j * F:(j + 1) * F],
                   ca_s.at[0], ca_r.at[g, j], me, tp).wait_recv()
        for j in range(1, NY):
            f = slice((j - 1) * F, j * F)
            ysend[r, f] = (part[r, cols_of(y_at(j) * 2 + c)].astype(f32)
                           + cxr[r, j * F:(j + 1) * F].astype(f32)).astype(bf16)
            send(ysend.at[r, f], yxr.at[r, f], yb_s.at[0], yb_r.at[g, j], me, y_at(j) * 2 + c)

    def give_back(g, k0, k1):
        r = pl.ds(k0 * C, (k1 - k0) * C)
        total = part[r, cols_of(tp)].astype(f32) + cxr[r, 0:F].astype(f32)
        for j in range(1, NY):
            f = slice((j - 1) * F, j * F)
            remote(ysend.at[r, f], yxr.at[r, f], yb_s.at[0], yb_r.at[g, j], me, tp).wait_recv()
            total = total + yxr[r, f].astype(f32)
        ret_send[r, :] = total.astype(bf16)
        for k in range(max(k0, 1), k1):
            send(ret_send.at[blk(k), :], ret_recv.at[blk(k), :], rb_s.at[0], rb_r.at[k], down_ep(k), tp)

    half = groups[0][1]
    done = 0
    for k in range(1, E):
        arrive(k)
        if k > 1:
            pass_on(k - 1)
    pass_on(E - 1)
    for cp in weight_copies:
        cp.wait()
    for k in range(1, E):
        complete(k)
    out_copies = [pltpu.make_async_copy(a, b, o_sem.at[i]) for i, (a, b) in enumerate(
        ((rows, rows_out), (cots, cots_out), (act, act_out), (dg, dg_out), (du, du_out)))]
    for cp in out_copies[:2]:
        cp.start()
    for g, (k0, k1) in enumerate(groups):
        experts(k0, k1)
        row_term(g, k0, k1)
        if g > 0:
            chip_sum(g - 1, *groups[g - 1])
    for cp in out_copies[2:]:
        cp.start()
    for j in range(1, NTP):
        send(sh_part, shx.at[j], sa_s.at[0], sa_r.at[j], me, lax.rem(tp + j, NTP))
    last = len(groups) - 1
    chip_sum(last, *groups[last])
    for j in range(1, NTP):
        remote(sh_part, shx.at[j], sa_s.at[0], sa_r.at[j], me, tp).wait_recv()
    tot = sh_part[:, :, 0:C]
    for j in range(1, NTP):
        tot = tot + shx[j, :, :, 0:C]
    sh_tot[:, :, 0:C] = tot
    for k in range(1, E):
        send(sh_tot.at[k], shr.at[k], sb_s.at[0], sb_r.at[k], down_ep(k), tp)
    for g, (k0, k1) in enumerate(groups):
        give_back(g, k0, k1)
    srow = lax.broadcasted_iota(jnp.int32, (E, T), 0)
    share = jnp.zeros((E, T), f32)
    for k in range(E):
        if k == 0:
            sv = sh_tot[0, :, 0:C]
        else:
            remote(sh_tot.at[k], shr.at[k], sb_s.at[0], sb_r.at[k], me, tp).wait_recv()
            sv = shr[k, :, 0:C]
        got = jnp.dot(sv, dsp[blk(k), :].astype(f32), precision=HIGH, preferred_element_type=f32)
        share = jnp.where(srow == k, got[0:1, :], share)
    d_rel = share - weight * jnp.sum(share, axis=0, keepdims=True)
    d_rel = jnp.where(hot, d_rel, 0.0)
    d_abs = lax.dot_general(perm, d_rel, (((0,), (0,)), ((), ())), precision=HIGH,
                            preferred_element_type=f32)
    rp_part[...] = jnp.dot(d_abs, tok_cols.astype(f32), precision=HIGH, preferred_element_type=f32)
    for k in range(1, E):
        send(rp_part, rpr.at[k], rp_s.at[0], rp_r.at[k], up_ep(k), tp)
    from_router = lax.dot_general(
        d_abs, rout[:, cols_of(tp)].astype(f32), (((0,), (0,)), ((), ())), precision=HIGH,
        preferred_element_type=f32)
    ret_recv[0:C, :] = ret_send[0:C, :]
    for k in range(1, E):
        remote(ret_send.at[blk(k), :], ret_recv.at[blk(k), :], rb_s.at[0], rb_r.at[k], me, tp).wait_recv()
    from_experts = lax.dot_general(dsp[...], ret_recv[...], (((0,), (0,)), ((), ())),
                                   preferred_element_type=f32)
    gtok_out[...] = (from_experts + from_router).astype(bf16)
    rsum = rp_part[...]
    for k in range(1, E):
        remote(rp_part, rpr.at[k], rp_s.at[0], rp_r.at[k], me, tp).wait_recv()
        rsum = rsum + rpr[k]
    grt_out[...] = rsum
    for cp in sends:
        cp.wait_send()
    for cp in out_copies:
        cp.wait()


def on_device(tokens, routes, router, w_gate, w_up, w_down, cotangent):
    E = lax.axis_size("ep")
    NTP = lax.axis_size("tp")
    NY = NTP // 2
    T, D = tokens.shape
    H = w_gate.shape[2]
    F = D // NTP
    capacity = 3 * T * routes.shape[1] // (2 * E)
    C = -(-capacity // 16) * 16
    R = E * C
    groups = ((0, E // 2), (E // 2, E))
    G = len(groups)
    bf16, f32 = jnp.bfloat16, jnp.float32
    V = pltpu.VMEM
    dma = pltpu.SemaphoreType.DMA
    vmem = pl.BlockSpec(memory_space=pltpu.VMEM)
    hbm = pl.BlockSpec(memory_space=pl.ANY)
    gtok, grt, rows, cots, act, dg, du = pl.pallas_call(
        functools.partial(kernel, (E, NTP, NY, C, T, D, F, H, groups)),
        out_shape=[
            jax.ShapeDtypeStruct((T, F), bf16), jax.ShapeDtypeStruct((E, F), f32),
            jax.ShapeDtypeStruct((R, D), bf16), jax.ShapeDtypeStruct((R, D), bf16),
            jax.ShapeDtypeStruct((R, H), bf16), jax.ShapeDtypeStruct((R, H), bf16),
            jax.ShapeDtypeStruct((R, H), bf16)],
        in_specs=[vmem, vmem, vmem, vmem, hbm, hbm, hbm],
        out_specs=[vmem, vmem, hbm, hbm, hbm, hbm, hbm],
        scratch_shapes=[
            V((D, H), bf16), V((D, H), bf16), V((H, D), bf16),
            V((R, T), bf16), V((R, F), bf16), V((R, F), bf16),
            V((R, D), bf16), V((R, D), bf16),
            V((R, H), bf16), V((R, H), bf16), V((R, H), bf16),
            V((R, D), bf16), V((R, NY * F), bf16),
            V((R, max(NY - 1, 1) * F), bf16), V((R, max(NY - 1, 1) * F), bf16),
            V((R, F), bf16), V((R, F), bf16),
            V((E, 8, 128), f32), V((NTP, E, 8, 128), f32), V((E, 8, 128), f32), V((E, 8, 128), f32),
            V((E, F), f32), V((E, E, F), f32),
            dma((3,)), dma((5,)), dma((2,)), dma((2, E)), dma((1,)), dma((2, E, NY)),
            dma((1,)), dma((2, E, NY)),
            dma((1,)), dma((G, NY)), dma((1,)), dma((G, NY)), dma((1,)), dma((E,)),
            dma((1,)), dma((NTP,)), dma((1,)), dma((E,)), dma((1,)), dma((E,)),
        ],
        compiler_params=pltpu.CompilerParams(
            collective_id=0, has_side_effects=True, vmem_limit_bytes=60 * 1024 * 1024),
    )(tokens, routes.T, router.T, cotangent, w_gate[0], w_up[0], w_down[0])
    tn = (((0,), (0,)), ((), ()))
    grad_gate = lax.dot_general(rows, dg, tn, preferred_element_type=f32)[None]
    grad_up = lax.dot_general(rows, du, tn, preferred_element_type=f32)[None]
    grad_down = lax.dot_general(act, cots, tn, preferred_element_type=f32)[None]
    return (gtok, grt.T, grad_gate, grad_up, grad_down)


def solution(mesh):
    return jax.shard_map(
        on_device,
        mesh=mesh,
        in_specs=(
            P("ep", None),
            P("ep", None),
            P(),
            P("ep", None, "tp"),
            P("ep", None, "tp"),
            P("ep", "tp", None),
            P("ep", None),
        ),
        out_specs=(
            P("ep", "tp"),
            P("tp", None),
            P("ep", None, "tp"),
            P("ep", None, "tp"),
            P("ep", "tp", None),
        ),
        check_vma=False,
    )
```

time: 159 us -> 82.5 us (0.52)
  blocking collectives: 78.5 us -> 0 us
  Pallas kernels: 0 us -> 68.8 us
  waiting for transfers between devices: 21.2 us -> 0 us
  matrix products: 29.4 us -> 11.5 us
  between operations: 13.9 us -> 0.68 us
  starting transfers between devices: 11.3 us -> 0 us
  other arithmetic: 1.9 us -> 0 us
  local copies, waits for them, and re-layouts: 2.9 us -> 1.28 us
    pallas_call x0 -> x1, Pallas kernels: none -> 68.8 us  [on_device(): pl.pallas_call(functools.partial(kernel, (E, NTP, NY, C, T, D, F, H, grou...]
    psum x2 -> x0, blocking collectives: 44.1 us -> none  [the longest x1 38.3 us: on_device(): grad_router = lax.psum(router_part, 'ep')]
    all_to_all x2 -> x0, blocking collectives: 34.3 us -> none  [the longest x1 19.2 us: on_device(): lax.all_to_all(token_slots.reshape(buffer_shape + (feature_part,)), 'ep',...]
    dot_general x14 -> x3, matrix products: 29.4 us -> 11.5 us  [the longest x1 4.91 us: on_device(): grad_gate = lax.dot_general(rows, dg, tn, preferred_element_type=f32)[None]]
    all_gather x2 -> x0, waiting for transfers between devices: 16.9 us -> none  [the longest x1 15.3 us: on_device(): lax.all_gather(sent_cot, 'tp', axis=3, tiled=True)]
    all_to_all x2 -> x0, starting transfers between devices: 11.2 us -> none  [the longest x1 5.67 us: on_device(): lax.all_to_all(share_sum[None].astype(jnp.bfloat16), 'ep', split_axis=1,...]
    reduce_scatter x1 -> x0, waiting for transfers between devices: 4.19 us -> none  [on_device(): lax.psum_scatter((row_term + jnp.einsum('ldf,slcf->dslc', w_up, d_up, pre...]
  transfers between devices with their start and end apart: 5 -> 0, of which waited for: 3 -> 0; matrix products, arithmetic and copies ran while one was open for 13% -> 0% of each run, Pallas kernels for 0% -> 0%
where the time goes in v1:
time: 82.5 us; the launch traced here: 82.3 us
  Pallas kernels  68.8 us (83%)
  matrix products  11.5 us (14%)
  local copies, waits for them, and re-layouts  1.28 us (2%)
    pallas_call x1, Pallas kernels, on_device(): pl.pallas_call(functools.partial(kernel, (E, NTP, NY, C, T, D, F, H, grou...  68.8 us
    dot_general x1, matrix products, on_device(): grad_gate = lax.dot_general(rows, dg, tn, preferred_element_type=f32)[None]  4.91 us
    dot_general x1, matrix products, on_device(): grad_up = lax.dot_general(rows, du, tn, preferred_element_type=f32)[None]  3.32 us
    dot_general x1, matrix products, on_device(): grad_down = lax.dot_general(act, cots, tn, preferred_element_type=f32)[None]  3.3 us

profile of v1, /device:TPU:0, one launch (start us, length us, event | category | flops | bytes accessed | tf_op | source)
XLA Modules:
  0.0 82.3 jit_solution(4051613175332916116)
XLA Ops:
  0.6 68.8 %shard_map.110 = (bf16[128,512]{1,0:T(8,128)(2,1)}, f32[8,512]{1,0:T(8,128)}, bf16[384,2048]{1,0:T(8,128)(2,1)}, bf16[384,2048]{1,0:T(8,128)(2,1)}, bf16[384,512...) custom-call(bf16[128,2048]{1,0:T(8,128)(2,1)} %tok.1, s32[2,128]{1,0:T(2,128)} %bitcast.23, ...), custom_call_target="tpu_custom_call" | custom-call | tf_op jit(solution)/shard_map/pallas_call | solution.py:288
  69.5 0.0 copy-start
  69.5 0.0 copy-start.3
  69.5 4.9 %convolution_bitcast_fusion.2 = f32[1,2048,512]{2,1,0:T(8,128)} fusion(bf16[384,2048]{1,0:T(8,128)(2,1)} %get-tuple-element.14, bf16[384,512]{1,0:T(8,128)(2,1)} %get-tuple-element.15), kind=kOutput, calls=%fused_computation.2 | convolution fusion | flops 805306368 | bytes 6160384 | tf_op jit(solution)/shard_map/dot_general | solution.py:316
  74.4 0.0 copy-done
  74.4 0.0 copy-done.3
  74.4 0.0 copy-start.1
  74.4 0.0 copy-start.2
  74.4 3.3 %convolution_bitcast_fusion.1 = f32[1,2048,512]{2,1,0:T(8,128)} fusion(bf16[384,2048]{1,0:T(8,128)(2,1)S(1)} %copy-done, bf16[384,512]{1,0:T(8,128)(2,1)S(1)} %copy-done.3), kind=kOutput, calls=%fused_computation.1 | convolution fusion | flops 805306368 | bytes 6160384 | tf_op jit(solution)/shard_map/dot_general | solution.py:317
  77.7 0.0 copy-done.1
  77.7 0.0 copy-done.2
  77.7 0.0 copy-start.4
  77.7 0.0 copy-start.5
  77.8 3.3 %convolution_bitcast_fusion = f32[1,512,2048]{2,1,0:T(8,128)} fusion(bf16[384,512]{1,0:T(8,128)(2,1)S(1)} %copy-done.2, bf16[384,2048]{1,0:T(8,128)(2,1)S(1)} %copy-done.1), kind=kOutput, calls=%fused_computation | convolution fusion | flops 805306368 | bytes 6160384 | tf_op jit(solution)/shard_map/dot_general | solution.py:318
  81.1 0.0 copy-done.4
  81.1 0.7 copy.14
  81.7 0.0 copy-done.5
  81.7 0.6 copy.15
Async XLA Ops:
  69.5 4.9 %copy-start = (bf16[384,2048]{1,0:T(8,128)(2,1)S(1)}, bf16[384,2048]{1,0:T(8,128)(2,1)}, u32[]{:S(2)}) copy-start(bf16[384,2048]{1,0:T(8,128)(2,1)} %get-tuple-element.14) | copy-start | bytes 4718596
  69.5 4.9 %copy-start.3 = (bf16[384,512]{1,0:T(8,128)(2,1)S(1)}, bf16[384,512]{1,0:T(8,128)(2,1)}, u32[]{:S(2)}) copy-start(bf16[384,512]{1,0:T(8,128)(2,1)} %get-tuple-element.16) | copy-start | bytes 1179652
  74.4 3.3 %copy-start.1 = (bf16[384,2048]{1,0:T(8,128)(2,1)S(1)}, bf16[384,2048]{1,0:T(8,128)(2,1)}, u32[]{:S(2)}) copy-start(bf16[384,2048]{1,0:T(8,128)(2,1)} %get-tuple-element.18) | copy-start | bytes 4718596
  74.4 3.3 %copy-start.2 = (bf16[384,512]{1,0:T(8,128)(2,1)S(1)}, bf16[384,512]{1,0:T(8,128)(2,1)}, u32[]{:S(2)}) copy-start(bf16[384,512]{1,0:T(8,128)(2,1)} %get-tuple-element.17) | copy-start | bytes 1179652
  77.7 3.3 %copy-start.4 = (bf16[128,512]{1,0:T(8,128)(2,1)S(1)}, bf16[128,512]{1,0:T(8,128)(2,1)}, u32[]{:S(2)}) copy-start(bf16[128,512]{1,0:T(8,128)(2,1)} %get-tuple-element.24) | copy-start | bytes 393220
  77.7 4.0 %copy-start.5 = (f32[8,512]{1,0:T(8,128)S(1)}, f32[8,512]{1,0:T(8,128)}, u32[]{:S(2)}) copy-start(f32[8,512]{1,0:T(8,128)} %get-tuple-element.13) | copy-start | bytes 49156

commit v2 on v1

--- a/solution.py
+++ b/solution.py
@@ -17,8 +17,8 @@
 def kernel(
     sizes,
     tok, rt, rout, cot, wg_hbm, wu_hbm, wd_hbm,
-    gtok_out, grt_out, rows_out, cots_out, act_out, dg_out, du_out,
-    wg, wu, wd, dsp, tok_send, cot_send, rows, cots, act, dg, du,
+    gtok_out, grt_out, rowst_out, cots_out, actt_out, dg_out, du_out,
+    wg, wu, wd, dsp, tok_send, cot_send, rows, cots, rowst, actt, act, cg, cu, dg, du,
     part, cxr, ysend, yxr, ret_send, ret_recv,
     sh_part, shx, sh_tot, shr, rp_part, rpr,
     w_sem, o_sem, ep_s, ep_r, y_s, y_r, c_s, c_r,
@@ -111,67 +111,73 @@
     bufs = (rows, cots)
     srcs = (tok_send, cot_send)
 
-    def arrive(k):
-        for a in range(2):
-            buf = bufs[a]
-            here = buf.at[blk(k), cols_of(tp)]
-            remote(srcs[a].at[blk(k), :], here, ep_s.at[a], ep_r.at[a, k], me, tp).wait_recv()
-            for j in range(1, NY):
-                send(here, here, y_s.at[0], y_r.at[a, k, j], me, y_at(j) * 2 + c)
-            send(here, here, c_s.at[0], c_r.at[a, k, 0], me, y * 2 + (1 - c))
-
-    def pass_on(k):
-        for a in range(2):
-            for j in range(1, NY):
-                t = lax.rem(y + (NY - j), NY) * 2 + c
-                here = bufs[a].at[blk(k), cols_of(t)]
-                remote(here, here, y_s.at[0], y_r.at[a, k, j], me, tp).wait_recv()
-                send(here, here, c_s.at[0], c_r.at[a, k, j], me, y * 2 + (1 - c))
-
-    def complete(k):
-        for a in range(2):
-            for j in range(NY):
-                t = lax.rem(y + (NY - j), NY) * 2 + (1 - c)
-                here = bufs[a].at[blk(k), cols_of(t)]
-                remote(here, here, c_s.at[0], c_r.at[a, k, j], me, tp).wait_recv()
-
-    tile = min(H, 256)
-    ones = jnp.ones((8, tile), f32)
-
-    def experts(k0, k1):
+    def arrive(a, k):
+        here = bufs[a].at[blk(k), cols_of(tp)]
+        remote(srcs[a].at[blk(k), :], here, ep_s.at[a], ep_r.at[a, k], me, tp).wait_recv()
+        for j in range(1, NY):
+            send(here, here, y_s.at[0], y_r.at[a, k, j], me, y_at(j) * 2 + c)
+        send(here, here, c_s.at[0], c_r.at[a, k, 0], me, y * 2 + (1 - c))
+
+    def pass_on(a, k):
+        for j in range(1, NY):
+            t = lax.rem(y + (NY - j), NY) * 2 + c
+            here = bufs[a].at[blk(k), cols_of(t)]
+            remote(here, here, y_s.at[0], y_r.at[a, k, j], me, tp).wait_recv()
+            send(here, here, c_s.at[0], c_r.at[a, k, j], me, y * 2 + (1 - c))
+
+    def complete(a, k):
+        for j in range(NY):
+            t = lax.rem(y + (NY - j), NY) * 2 + (1 - c)
+            here = bufs[a].at[blk(k), cols_of(t)]
+            remote(here, here, c_s.at[0], c_r.at[a, k, j], me, tp).wait_recv()
+
+    tile = min(H, 128)
+
+    def forward(n):
+        cn = slice(n, n + tile)
+        pre_gate = jnp.dot(rows[...], wg[:, cn], preferred_element_type=f32)
+        pre_up = jnp.dot(rows[...], wu[:, cn], preferred_element_type=f32)
+        g = jnp.minimum(pre_gate, clamp_limit)
+        u1 = jnp.clip(pre_up, -clamp_limit, clamp_limit) + 1.0
+        sg = jax.nn.sigmoid(sig_slope * g)
+        ga = g * sg
+        a = (u1 * ga).astype(bf16)
+        act[:, cn] = a
+        actt[cn, :] = a.T
+        slope = sg + sig_slope * ga * (1.0 - sg)
+        cg[:, cn] = jnp.where(pre_gate < clamp_limit, u1 * slope, 0.0)
+        cu[:, cn] = jnp.where(jnp.abs(pre_up) < clamp_limit, ga, 0.0)
+
+    def backward(g, k0, k1):
         r = pl.ds(k0 * C, (k1 - k0) * C)
-        sums = [jnp.zeros((8, C), f32) for _ in range(k0, k1)]
+        total = None
         for n in range(0, H, tile):
             cn = slice(n, n + tile)
-            pre_gate = jnp.dot(rows[r, :], wg[:, cn], preferred_element_type=f32)
-            pre_up = jnp.dot(rows[r, :], wu[:, cn], preferred_element_type=f32)
             back = lax.dot_general(cots[r, :], wd[cn, :], NT, preferred_element_type=f32)
-            g = jnp.minimum(pre_gate, clamp_limit)
-            u1 = jnp.clip(pre_up, -clamp_limit, clamp_limit) + 1.0
-            sg = jax.nn.sigmoid(sig_slope * g)
-            ga = g * sg
-            a = (u1 * ga).astype(bf16)
-            act[r, cn] = a
-            prod = a.astype(f32) * back
-            slope = sg + sig_slope * ga * (1.0 - sg)
-            dg[r, cn] = jnp.where(pre_gate < clamp_limit, back * u1 * slope, 0.0).astype(bf16)
-            du[r, cn] = jnp.where(jnp.abs(pre_up) < clamp_limit, back * ga, 0.0).astype(bf16)
-            for i in range(k1 - k0):
-                sums[i] = sums[i] + lax.dot_general(
-                    ones, prod[i * C:(i + 1) * C, :], NT, precision=HIGH, preferred_element_type=f32)
-        for i in range(k1 - k0):
-            sh_part[k0 + i, :, 0:C] = sums[i]
+            dg[r, cn] = (back * cg[r, cn]).astype(bf16)
+            du[r, cn] = (back * cu[r, cn]).astype(bf16)
+            prod = act[r, cn].astype(f32) * back
+            total = prod if total is None else total + prod
+        sh_part[g, :, 0:(k1 - k0) * C] = lax.dot_general(
+            jnp.ones((8, tile), f32), total, NT, precision=HIGH, preferred_element_type=f32)
 
     def row_term(g, k0, k1):
         r = pl.ds(k0 * C, (k1 - k0) * C)
-        for n in range(0, D, 512):
-            part[r, n:n + 512] = (
-                lax.dot_general(dg[r, :], wg[n:n + 512, :], NT, preferred_element_type=f32)
-                + lax.dot_general(du[r, :], wu[n:n + 512, :], NT, preferred_element_type=f32)
+
+        def piece(t):
+            d = pl.ds(pl.multiple_of(t * F, F), F)
+            part[r, d] = (
+                lax.dot_general(dg[r, :], wg[d, :], NT, preferred_element_type=f32)
+                + lax.dot_general(du[r, :], wu[d, :], NT, preferred_element_type=f32)
             ).astype(bf16)
-        for j in range(NY):
+
+        order = list(range(1, NY)) + [0]
+        for j in order:
+            piece(y_at(j) * 2 + (1 - c))
             send(part.at[r, cols_of(y_at(j) * 2 + (1 - c))], cxr.at[r, j * F:(j + 1) * F],
                  ca_s.at[0], ca_r.at[g, j], me, y * 2 + (1 - c))
+        for j in order:
+            piece(y_at(j) * 2 + c)
 
     def chip_sum(g, k0, k1):
         r = pl.ds(k0 * C, (k1 - k0) * C)
@@ -195,38 +201,53 @@
         for k in range(max(k0, 1), k1):
             send(ret_send.at[blk(k), :], ret_recv.at[blk(k), :], rb_s.at[0], rb_r.at[k], down_ep(k), tp)
 
-    half = groups[0][1]
-    done = 0
-    for k in range(1, E):
-        arrive(k)
-        if k > 1:
-            pass_on(k - 1)
-    pass_on(E - 1)
-    for cp in weight_copies:
-        cp.wait()
-    for k in range(1, E):
-        complete(k)
     out_copies = [pltpu.make_async_copy(a, b, o_sem.at[i]) for i, (a, b) in enumerate(
-        ((rows, rows_out), (cots, cots_out), (act, act_out), (dg, dg_out), (du, du_out)))]
-    for cp in out_copies[:2]:
-        cp.start()
+        ((rowst, rowst_out), (actt, actt_out), (cots, cots_out), (dg, dg_out), (du, du_out)))]
+    items = [(a, k) for a in range(2) for k in range(1, E)]
+    tiles = list(range(0, H, tile))
+    per = max(1, -(-len(tiles) // max(1, E - 4)))
+    for i, (a, k) in enumerate(items):
+        arrive(a, k)
+        if i > 0:
+            pass_on(*items[i - 1])
+        if (a, k) == (1, min(2, E - 1)):
+            for cp in weight_copies:
+                cp.wait()
+            for kk in range(1, E):
+                complete(0, kk)
+        if a == 1 and k >= min(2, E - 1):
+            for n in tiles[:per]:
+                forward(n)
+            tiles = tiles[per:]
+    pass_on(*items[-1])
+    for n in tiles:
+        forward(n)
+    nt = min(D, 256)
+    for n in range(0, D, nt):
+        rowst[n:n + nt, :] = rows[:, n:n + nt].T
+    out_copies[0].start()
+    out_copies[1].start()
     for g, (k0, k1) in enumerate(groups):
-        experts(k0, k1)
+        for k in range(max(k0, 1), k1):
+            complete(1, k)
+        backward(g, k0, k1)
         row_term(g, k0, k1)
         if g > 0:
             chip_sum(g - 1, *groups[g - 1])
     for cp in out_copies[2:]:
         cp.start()
+    last = len(groups) - 1
     for j in range(1, NTP):
         send(sh_part, shx.at[j], sa_s.at[0], sa_r.at[j], me, lax.rem(tp + j, NTP))
-    last = len(groups) - 1
     chip_sum(last, *groups[last])
     for j in range(1, NTP):
         remote(sh_part, shx.at[j], sa_s.at[0], sa_r.at[j], me, tp).wait_recv()
-    tot = sh_part[:, :, 0:C]
-    for j in range(1, NTP):
-        tot = tot + shx[j, :, :, 0:C]
-    sh_tot[:, :, 0:C] = tot
+    for g, (k0, k1) in enumerate(groups):
+        tot = sh_part[g, :, 0:(k1 - k0) * C]
+        for j in range(1, NTP):
+            tot = tot + shx[j, g, :, 0:(k1 - k0) * C]
+        for k in range(k0, k1):
+            sh_tot[k, :, 0:C] = tot[:, (k - k0) * C:(k - k0 + 1) * C]
     for k in range(1, E):
         send(sh_tot.at[k], shr.at[k], sb_s.at[0], sb_r.at[k], down_ep(k), tp)
     for g, (k0, k1) in enumerate(groups):
@@ -268,6 +289,13 @@
         cp.wait()
 
 
+def weight_grads(rowst, dg, du, actt, cots, gate_out, up_out, down_out):
+    f32 = jnp.float32
+    gate_out[0] = jnp.dot(rowst[...], dg[...], preferred_element_type=f32)
+    up_out[0] = jnp.dot(rowst[...], du[...], preferred_element_type=f32)
+    down_out[0] = jnp.dot(actt[...], cots[...], preferred_element_type=f32)
+
+
 def on_device(tokens, routes, router, w_gate, w_up, w_down, cotangent):
     E = lax.axis_size("ep")
     NTP = lax.axis_size("tp")
@@ -280,29 +308,30 @@
     R = E * C
     groups = ((0, E // 2), (E // 2, E))
     G = len(groups)
+    SW = -(-max(b - a for a, b in groups) * C // 128) * 128
     bf16, f32 = jnp.bfloat16, jnp.float32
     V = pltpu.VMEM
     dma = pltpu.SemaphoreType.DMA
     vmem = pl.BlockSpec(memory_space=pltpu.VMEM)
     hbm = pl.BlockSpec(memory_space=pl.ANY)
-    gtok, grt, rows, cots, act, dg, du = pl.pallas_call(
+    gtok, grt, rowst, cots, actt, dg, du = pl.pallas_call(
         functools.partial(kernel, (E, NTP, NY, C, T, D, F, H, groups)),
         out_shape=[
             jax.ShapeDtypeStruct((T, F), bf16), jax.ShapeDtypeStruct((E, F), f32),
-            jax.ShapeDtypeStruct((R, D), bf16), jax.ShapeDtypeStruct((R, D), bf16),
-            jax.ShapeDtypeStruct((R, H), bf16), jax.ShapeDtypeStruct((R, H), bf16),
+            jax.ShapeDtypeStruct((D, R), bf16), jax.ShapeDtypeStruct((R, D), bf16),
+            jax.ShapeDtypeStruct((H, R), bf16), jax.ShapeDtypeStruct((R, H), bf16),
             jax.ShapeDtypeStruct((R, H), bf16)],
         in_specs=[vmem, vmem, vmem, vmem, hbm, hbm, hbm],
         out_specs=[vmem, vmem, hbm, hbm, hbm, hbm, hbm],
         scratch_shapes=[
             V((D, H), bf16), V((D, H), bf16), V((H, D), bf16),
             V((R, T), bf16), V((R, F), bf16), V((R, F), bf16),
-            V((R, D), bf16), V((R, D), bf16),
-            V((R, H), bf16), V((R, H), bf16), V((R, H), bf16),
+            V((R, D), bf16), V((R, D), bf16), V((D, R), bf16), V((H, R), bf16),
+            V((R, H), bf16), V((R, H), f32), V((R, H), f32), V((R, H), bf16), V((R, H), bf16),
             V((R, D), bf16), V((R, NY * F), bf16),
             V((R, max(NY - 1, 1) * F), bf16), V((R, max(NY - 1, 1) * F), bf16),
             V((R, F), bf16), V((R, F), bf16),
-            V((E, 8, 128), f32), V((NTP, E, 8, 128), f32), V((E, 8, 128), f32), V((E, 8, 128), f32),
+            V((G, 8, SW), f32), V((NTP, G, 8, SW), f32), V((E, 8, 128), f32), V((E, 8, 128), f32),
             V((E, F), f32), V((E, E, F), f32),
             dma((3,)), dma((5,)), dma((2,)), dma((2, E)), dma((1,)), dma((2, E, NY)),
             dma((1,)), dma((2, E, NY)),
@@ -312,10 +341,22 @@
         compiler_params=pltpu.CompilerParams(
             collective_id=0, has_side_effects=True, vmem_limit_bytes=60 * 1024 * 1024),
     )(tokens, routes.T, router.T, cotangent, w_gate[0], w_up[0], w_down[0])
-    tn = (((0,), (0,)), ((), ()))
-    grad_gate = lax.dot_general(rows, dg, tn, preferred_element_type=f32)[None]
-    grad_up = lax.dot_general(rows, du, tn, preferred_element_type=f32)[None]
-    grad_down = lax.dot_general(act, cots, tn, preferred_element_type=f32)[None]
+    steps = 8
+    dt, ht = D // steps, H // steps
+    grad_gate, grad_up, grad_down = pl.pallas_call(
+        weight_grads,
+        grid=(steps,),
+        out_shape=[jax.ShapeDtypeStruct((1, D, H), f32), jax.ShapeDtypeStruct((1, D, H), f32),
+                   jax.ShapeDtypeStruct((1, H, D), f32)],
+        in_specs=[
+            pl.BlockSpec((dt, R), lambda i: (i, 0)), pl.BlockSpec((R, H), lambda i: (0, 0)),
+            pl.BlockSpec((R, H), lambda i: (0, 0)), pl.BlockSpec((ht, R), lambda i: (i, 0)),
+            pl.BlockSpec((R, D), lambda i: (0, 0))],
+        out_specs=[
+            pl.BlockSpec((1, dt, H), lambda i: (0, i, 0)), pl.BlockSpec((1, dt, H), lambda i: (0, i, 0)),
+            pl.BlockSpec((1, ht, D), lambda i: (0, i, 0))],
+        compiler_params=pltpu.CompilerParams(dimension_semantics=("arbitrary",)),
+    )(rowst, dg, du, actt, cots)
     return (gtok, grt.T, grad_gate, grad_up, grad_down)
 
 

time: 82.5 us -> 82.7 us (level)
  Pallas kernels: 68.8 us -> 80.5 us
  matrix products: 11.5 us -> 0 us
    dot_general x3 -> x0, matrix products: 11.5 us -> none  [the longest x1 4.91 us: on_device(): grad_gate = lax.dot_general(rows, dg, tn, preferred_element_type=f32)[None]]
    pallas_call x0 -> x1, Pallas kernels: none -> 9.4 us  [on_device(): pl.pallas_call(weight_grads, grid=(steps,), out_shape=[jax.ShapeDtypeStru...]
    pallas_call x1, Pallas kernels: 68.8 us -> 71.1 us  [on_device(): pl.pallas_call(functools.partial(kernel, (E, NTP, NY, C, T, D, F, H, grou...]
where the time goes in v2:
time: 82.7 us; the launch traced here: 82.4 us
  Pallas kernels  80.5 us (97%)
  local copies, waits for them, and re-layouts  1.27 us (2%)
    pallas_call x1, Pallas kernels, on_device(): pl.pallas_call(functools.partial(kernel, (E, NTP, NY, C, T, D, F, H, grou...  71.1 us
    pallas_call x1, Pallas kernels, on_device(): pl.pallas_call(weight_grads, grid=(steps,), out_shape=[jax.ShapeDtypeStru...  9.4 us

profile of v2, /device:TPU:0, one launch (start us, length us, event | category | flops | bytes accessed | tf_op | source)
XLA Modules:
  0.0 82.4 jit_solution(10984650566707694921)
XLA Ops:
  0.6 71.1 %shard_map.110 = (bf16[128,512]{1,0:T(8,128)(2,1)}, f32[8,512]{1,0:T(8,128)}, bf16[2048,384]{1,0:T(8,128)(2,1)}, bf16[384,2048]{1,0:T(8,128)(2,1)}, bf16[512,384...) custom-call(bf16[128,2048]{1,0:T(8,128)(2,1)} %tok.1, s32[2,128]{1,0:T(2,128)} %bitcast.11, ...), custom_call_target="tpu_custom_call" | custom-call | tf_op jit(solution)/shard_map/pallas_call | solution.py:317
  71.7 0.0 copy-start
  71.8 0.0 copy-start.1
  71.8 9.4 %shard_map.111 = (f32[1,2048,512]{2,1,0:T(8,128)}, f32[1,2048,512]{2,1,0:T(8,128)}, f32[1,512,2048]{2,1,0:T(8,128)}) custom-call(bf16[2048,384]{1,0:T(8,128)(2,1)} %get-tuple-element.17.rowst, bf16[384,512]{1,0:T(8,128)(2,1)} %get-tuple-element.18.dg, bf16[384,512]{1,0:T(8,128)(2,1)} %get-tuple-element.19.du, bf16[512,384]{1,0:T(8,128)(2,1)} %get-tuple-element.20.actt, ...), custom_call_target="tpu_custom_call" | custom-call | tf_op jit(solution)/shard_map/pallas_call | solution.py:346
  81.2 0.0 copy-done
  81.2 0.7 copy.14
  81.8 0.0 copy-done.1
  81.8 0.6 copy.15
Async XLA Ops:
  71.7 9.4 %copy-start = (bf16[128,512]{1,0:T(8,128)(2,1)S(1)}, bf16[128,512]{1,0:T(8,128)(2,1)}, u32[]{:S(2)}) copy-start(bf16[128,512]{1,0:T(8,128)(2,1)} %get-tuple-element.30) | copy-start | bytes 393220
  71.8 10.1 %copy-start.1 = (f32[8,512]{1,0:T(8,128)S(1)}, f32[8,512]{1,0:T(8,128)}, u32[]{:S(2)}) copy-start(f32[8,512]{1,0:T(8,128)} %get-tuple-element.16) | copy-start | bytes 49156

commit v3 on v2

--- a/solution.py
+++ b/solution.py
@@ -9,6 +9,7 @@
 
 clamp_limit = 7.0
 sig_slope = 1.702
+WINDOW = 3
 MESH = pl.DeviceIdType.MESH
 HIGH = lax.Precision.HIGHEST
 NT = (((1,), (1,)), ((), ()))
@@ -84,9 +85,17 @@
     def blk(k):
         return pl.ds(k * C, C)
 
-    for k in range(1, E):
-        send(tok_send.at[blk(k), :], rows.at[blk(k), cols_of(tp)],
-             ep_s.at[0], ep_r.at[0, k], up_ep(k), tp)
+    bufs = (rows, cots)
+    srcs = (tok_send, cot_send)
+    items = [(a, k) for a in range(2) for k in range(1, E)]
+    window = min(WINDOW, E - 1)
+
+    def send_out(a, k):
+        send(srcs[a].at[blk(k), :], bufs[a].at[blk(k), cols_of(tp)],
+             ep_s.at[a], ep_r.at[a, k], up_ep(k), tp)
+
+    for a, k in items[:window]:
+        send_out(a, k)
 
     perm = (lax.broadcasted_iota(jnp.int32, (E, E), 1)
             == lax.rem(lax.broadcasted_iota(jnp.int32, (E, E), 0) + me, E)).astype(f32)
@@ -102,14 +111,8 @@
     for k in list(range(1, E)):
         raw = jnp.dot(dsp[blk(k), :], cot_cols, preferred_element_type=f32)
         cot_send[blk(k), :] = (wcols[k] * raw).astype(bf16)
-    for k in range(1, E):
-        send(cot_send.at[blk(k), :], cots.at[blk(k), cols_of(tp)],
-             ep_s.at[1], ep_r.at[1, k], up_ep(k), tp)
     rows[0:C, :] = jnp.dot(dsp[0:C, :], tok[...], preferred_element_type=f32).astype(bf16)
     cots[0:C, :] = (wcols[0] * jnp.dot(dsp[0:C, :], cot[...], preferred_element_type=f32)).astype(bf16)
-
-    bufs = (rows, cots)
-    srcs = (tok_send, cot_send)
 
     def arrive(a, k):
         here = bufs[a].at[blk(k), cols_of(tp)]
@@ -203,11 +206,12 @@
 
     out_copies = [pltpu.make_async_copy(a, b, o_sem.at[i]) for i, (a, b) in enumerate(
         ((rowst, rowst_out), (actt, actt_out), (cots, cots_out), (dg, dg_out), (du, du_out)))]
-    items = [(a, k) for a in range(2) for k in range(1, E)]
     tiles = list(range(0, H, tile))
     per = max(1, -(-len(tiles) // max(1, E - 4)))
     for i, (a, k) in enumerate(items):
         arrive(a, k)
+        if i + window < len(items):
+            send_out(*items[i + window])
         if i > 0:
             pass_on(*items[i - 1])
         if (a, k) == (1, min(2, E - 1)):

time: 82.7 us -> 79.1 us (0.956)
  Pallas kernels: 80.5 us -> 76.8 us
    pallas_call x1, Pallas kernels: 71.1 us -> 67.4 us  [on_device(): pl.pallas_call(functools.partial(kernel, (E, NTP, NY, C, T, D, F, H, grou...]
where the time goes in v3:
time: 79.1 us; the launch traced here: 78.7 us
  Pallas kernels  76.8 us (97%)
  local copies, waits for them, and re-layouts  1.27 us (2%)
    pallas_call x1, Pallas kernels, on_device(): pl.pallas_call(functools.partial(kernel, (E, NTP, NY, C, T, D, F, H, grou...  67.4 us
    pallas_call x1, Pallas kernels, on_device(): pl.pallas_call(weight_grads, grid=(steps,), out_shape=[jax.ShapeDtypeStru...  9.4 us

profile of v3, /device:TPU:0, one launch (start us, length us, event | category | flops | bytes accessed | tf_op | source)
XLA Modules:
  0.0 78.7 jit_solution(13971340427033749850)
XLA Ops:
  0.6 67.4 %shard_map.110 = (bf16[128,512]{1,0:T(8,128)(2,1)}, f32[8,512]{1,0:T(8,128)}, bf16[2048,384]{1,0:T(8,128)(2,1)}, bf16[384,2048]{1,0:T(8,128)(2,1)}, bf16[512,384...) custom-call(bf16[128,2048]{1,0:T(8,128)(2,1)} %tok.1, s32[2,128]{1,0:T(2,128)} %bitcast.11, ...), custom_call_target="tpu_custom_call" | custom-call | tf_op jit(solution)/shard_map/pallas_call | solution.py:321
  68.0 0.0 copy-start
  68.1 0.0 copy-start.1
  68.1 9.4 %shard_map.111 = (f32[1,2048,512]{2,1,0:T(8,128)}, f32[1,2048,512]{2,1,0:T(8,128)}, f32[1,512,2048]{2,1,0:T(8,128)}) custom-call(bf16[2048,384]{1,0:T(8,128)(2,1)} %get-tuple-element.17.rowst, bf16[384,512]{1,0:T(8,128)(2,1)} %get-tuple-element.18.dg, bf16[384,512]{1,0:T(8,128)(2,1)} %get-tuple-element.19.du, bf16[512,384]{1,0:T(8,128)(2,1)} %get-tuple-element.20.actt, ...), custom_call_target="tpu_custom_call" | custom-call | tf_op jit(solution)/shard_map/pallas_call | solution.py:350
  77.5 0.0 copy-done
  77.5 0.7 copy.14
  78.1 0.0 copy-done.1
  78.1 0.6 copy.15
Async XLA Ops:
  68.0 9.4 %copy-start = (bf16[128,512]{1,0:T(8,128)(2,1)S(1)}, bf16[128,512]{1,0:T(8,128)(2,1)}, u32[]{:S(2)}) copy-start(bf16[128,512]{1,0:T(8,128)(2,1)} %get-tuple-element.30) | copy-start | bytes 393220
  68.1 10.1 %copy-start.1 = (f32[8,512]{1,0:T(8,128)S(1)}, f32[8,512]{1,0:T(8,128)}, u32[]{:S(2)}) copy-start(f32[8,512]{1,0:T(8,128)} %get-tuple-element.16) | copy-start | bytes 49156
